TPU v7x, 32 devices: a whole 2x2x4 slice. The times are simulated.
32 devices in a mesh: ep: 4 (over y, x), tp: 8 (over z, core).
Axes of the slice: x: 2, y: 2, z: 4, core: 2. Of those that a mesh axis runs over, the one named last changes fastest.
Arguments:
- tokens: bfloat16 [64, 2048], P('ep'), may hold values from -6 to 6
- routes: int32 [64, 4], P('ep'), may hold values from 0 to 7, all different within a row; in each aligned block of 16 rows (0 to 15, 16 to 31, ...) at most 16 rows name the same one
- route_weight: float32 [64, 4], P('ep'), may hold values from 0.2 to 1
- mixer_gain: float32 [2048], replicated, may hold values from 0.1 to 1.9
- gate_weight: bfloat16 [2048, 4096], P(None, 'tp'), may hold values from -0.125 to 0.125
- input_weight: bfloat16 [2048, 4096], P(None, 'tp'), may hold values from -0.125 to 0.125
- step_weight: bfloat16 [2048, 64], P(None, 'tp'), may hold values from -0.125 to 0.125
- write_weight: bfloat16 [2048, 512], P('tp'), may hold values from -0.125 to 0.125
- read_weight: bfloat16 [2048, 512], P('tp'), may hold values from -0.125 to 0.125
- step_bias: float32 [64], P('tp'), may hold values from -3 to 0.5
- decay_log: float32 [64], P('tp'), may hold values from -2 to 0.5
- decay_jolt: float32 [64, 64], P('ep', 'tp'), may hold values from -1 to 0
- filter_taps: bfloat16 [4, 4096], P(None, 'tp'), may hold values from -3 to 3
- filter_state: bfloat16 [64, 3, 4096], P('ep', None, 'tp'), may hold values from -6 to 6
- scan_state: float32 [64, 64, 64, 128], P('ep', 'tp'), may hold values from -2 to 2
- skip_gain: float32 [64], P('tp'), may hold values from 0.5 to 2
- head_gain: float32 [4096], P('tp'), may hold values from 0.1 to 1.9
- output_weight: bfloat16 [4096, 2048], P('tp'), may hold values from -0.09375 to 0.09375
- channel_gain: float32 [2048], replicated, may hold values from 0.1 to 1.9
- expert_gate: bfloat16 [8, 2048, 2048], P('ep', None, 'tp'), may hold values from -0.125 to 0.125
- expert_up: bfloat16 [8, 2048, 2048], P('ep', None, 'tp'), may hold values from -0.125 to 0.125
- expert_down: bfloat16 [8, 2048, 2048], P('ep', 'tp'), may hold values from -0.125 to 0.125
- shared_gate: bfloat16 [2048, 2048], P(None, 'tp'), may hold values from -0.125 to 0.125
- shared_up: bfloat16 [2048, 2048], P(None, 'tp'), may hold values from -0.125 to 0.125
- shared_down: bfloat16 [2048, 2048], P('tp'), may hold values from -0.125 to 0.125
Outputs:
- layer_out: bfloat16 [64, 2048], P('ep', 'tp')
- new_state: float32 [64, 64, 64, 128], P('ep', 'tp')
- new_filter: bfloat16 [64, 3, 4096], P('ep', None, 'tp')
Inputs may be any that keep to these rules, and one draw needn't show every extreme that they name: `routes`: each row names 4 different experts. In each aligned block of 16 rows (the rows of one index of ep) no expert is named by more than 16 rows, a bound that some block reaches.
All inputs are finite; a program needn't handle non-finite values.
Results may differ from a plain program's by a relative error of at most 0.025.
Values may be sent and summed in bfloat16 or wider, within the bound.
A program may use at most 64 MiB of HBM per device.

v0:
```python
import jax
import jax.numpy as jnp
from jax import lax
from jax.sharding import PartitionSpec as P

HEADS = 64
HEAD_DIM = 64
GROUPS = 4
STATE = 128


EPS = 1e-06


def rms_normed(values, scaling):
    mean_square = jnp.mean(values * values, axis=-1, keepdims=True)
    return values * lax.rsqrt(mean_square + EPS) * scaling


def route_targets(route_ids, experts, capacity):
    count_rows, top_picks = route_ids.shape
    flattened = route_ids.reshape(count_rows * top_picks)
    onehot = (flattened[:, None] == jnp.arange(experts, dtype=jnp.int32)[None, :]).astype(jnp.int32)
    before = jnp.cumsum(onehot, axis=0) - onehot
    slot_index = jnp.sum(before * onehot, axis=1)
    return (flattened * capacity + slot_index).reshape(count_rows, top_picks)


def expert_terms(token_rows, expert_gate, expert_up, expert_down):
    gate_part = jnp.einsum(
        "ajcd,jdf->ajcf", token_rows, expert_gate, preferred_element_type=jnp.float32
    )
    up_part = jnp.einsum(
        "ajcd,jdf->ajcf", token_rows, expert_up, preferred_element_type=jnp.float32
    )
    hidden = (jax.nn.silu(gate_part) * up_part).astype(jnp.bfloat16)
    return jnp.einsum("ajcf,jfd->ajcd", hidden, expert_down, preferred_element_type=jnp.float32)


def on_device(
    tokens,
    routes,
    route_weight,
    mixer_gain,
    gate_weight,
    input_weight,
    step_weight,
    write_weight,
    read_weight,
    step_bias,
    decay_log,
    decay_jolt,
    filter_taps,
    filter_state,
    scan_state,
    skip_gain,
    head_gain,
    output_weight,
    channel_gain,
    expert_gate,
    expert_up,
    expert_down,
    shared_gate,
    shared_up,
    shared_down,
):
    seq_rows, model_width = tokens.shape
    tp_count = lax.axis_size("tp")
    tp_index = lax.axis_index("tp")
    ep_count = lax.axis_size("ep")
    col_count = model_width // tp_count
    col_start = tp_index * col_count
    tokens_f = tokens.astype(jnp.float32)
    normed = rms_normed(tokens_f, mixer_gain).astype(jnp.bfloat16)
    feature_rows = write_weight.shape[0]
    own_features = lax.dynamic_slice_in_dim(normed, tp_index * feature_rows, feature_rows, 1)
    write_part = jnp.dot(own_features, write_weight, preferred_element_type=jnp.float32)
    read_part = jnp.dot(own_features, read_weight, preferred_element_type=jnp.float32)
    write_in, read_in = (
        lax.psum(write_part.astype(jnp.bfloat16), "tp").astype(jnp.float32),
        lax.psum(read_part.astype(jnp.bfloat16), "tp").astype(jnp.float32),
    )
    gate_rows = jnp.dot(normed, gate_weight, preferred_element_type=jnp.float32).astype(
        jnp.bfloat16
    )
    input_rows = jnp.dot(normed, input_weight, preferred_element_type=jnp.float32).astype(
        jnp.bfloat16
    )
    step_raw = jnp.dot(normed, step_weight, preferred_element_type=jnp.float32)
    window = jnp.concatenate([filter_state, input_rows[:, None, :]], axis=1)
    filtered = jax.nn.silu(
        jnp.sum(window.astype(jnp.float32) * filter_taps.astype(jnp.float32)[None], axis=1)
    )
    step_size = jax.nn.softplus(step_raw + step_bias)
    log_decay = decay_jolt - jnp.exp(decay_log) * step_size
    heads_here = step_bias.shape[0]
    head_input = filtered.reshape(seq_rows, heads_here, HEAD_DIM)
    group_index = tp_index * heads_here // (HEADS // GROUPS)
    write_vec = jax.nn.silu(lax.dynamic_slice_in_dim(write_in, group_index * STATE, STATE, 1))
    read_vec = jax.nn.silu(lax.dynamic_slice_in_dim(read_in, group_index * STATE, STATE, 1))
    new_state = (
        jnp.exp(log_decay)[:, :, None, None] * scan_state
        + (step_size[:, :, None] * head_input)[:, :, :, None] * write_vec[:, None, None, :]
    )
    readout = jnp.einsum("shpn,sn->shp", new_state, read_vec, precision=lax.Precision.HIGHEST)
    readout = readout + skip_gain[None, :, None] * head_input
    gate_heads = gate_rows.astype(jnp.float32).reshape(seq_rows, heads_here, HEAD_DIM)
    gated = rms_normed(readout * jax.nn.silu(gate_heads), head_gain.reshape(heads_here, HEAD_DIM))
    gated = gated.astype(jnp.bfloat16).reshape(seq_rows, heads_here * HEAD_DIM)
    mixer_part = jnp.dot(gated, output_weight, preferred_element_type=jnp.float32)
    mixed = lax.psum(mixer_part.astype(jnp.bfloat16), "tp")
    resid = (tokens_f + mixed.astype(jnp.float32)).astype(jnp.bfloat16)
    normed_ffn = rms_normed(resid.astype(jnp.float32), channel_gain).astype(jnp.bfloat16)
    resid_own = lax.dynamic_slice_in_dim(resid, col_start, col_count, 1)
    shared_hidden = (
        jax.nn.silu(jnp.dot(normed_ffn, shared_gate, preferred_element_type=jnp.float32))
        * jnp.dot(normed_ffn, shared_up, preferred_element_type=jnp.float32)
    ).astype(jnp.bfloat16)
    shared_part = jnp.dot(shared_hidden, shared_down, preferred_element_type=jnp.float32)
    local_experts = expert_gate.shape[0]
    experts = local_experts * ep_count
    top_picks = routes.shape[1]
    capacity = 2 * seq_rows * top_picks // experts
    targets = route_targets(routes, experts, capacity)
    slot_ids = jnp.arange(experts * capacity, dtype=jnp.int32)
    dispatch = jnp.sum((targets[None, :, :] == slot_ids[:, None, None]).astype(jnp.float32), axis=2)
    send_rows = jnp.dot(
        dispatch.astype(jnp.bfloat16), normed_ffn, preferred_element_type=jnp.float32
    )
    send_rows = send_rows.astype(jnp.bfloat16).reshape(
        ep_count, local_experts, capacity, model_width
    )
    terms = expert_terms(
        lax.all_to_all(send_rows, "ep", split_axis=0, concat_axis=0, tiled=True),
        expert_gate,
        expert_up,
        expert_down,
    )
    routed_parts, shared_sum = (
        lax.psum_scatter(terms.astype(jnp.bfloat16), "tp", scatter_dimension=3, tiled=True).astype(
            jnp.float32
        ),
        lax.psum_scatter(
            shared_part.reshape(1, 1, seq_rows, model_width).astype(jnp.bfloat16),
            "tp",
            scatter_dimension=3,
            tiled=True,
        ).astype(jnp.float32),
    )
    expert_rows = routed_parts.astype(jnp.bfloat16)
    returned = lax.all_to_all(expert_rows, "ep", split_axis=0, concat_axis=0, tiled=True)
    returned = returned.reshape(experts * capacity, col_count).astype(jnp.float32)
    combine = jnp.sum(
        jnp.where(targets[:, :, None] == slot_ids[None, None, :], route_weight[:, :, None], 0.0),
        axis=1,
    )
    routed_sum = jnp.dot(combine, returned, precision=lax.Precision.HIGHEST)
    layer_out = (resid_own.astype(jnp.float32) + shared_sum[0, 0] + routed_sum).astype(jnp.bfloat16)
    return (layer_out, new_state, window[:, 1:, :])


def solution(mesh):
    in_specs = (
        P("ep", None),
        P("ep", None),
        P("ep", None),
        P(),
        P(None, "tp"),
        P(None, "tp"),
        P(None, "tp"),
        P("tp", None),
        P("tp", None),
        P("tp"),
        P("tp"),
        P("ep", "tp"),
        P(None, "tp"),
        P("ep", None, "tp"),
        P("ep", "tp", None, None),
        P("tp"),
        P("tp"),
        P("tp", None),
        P(),
        P("ep", None, "tp"),
        P("ep", None, "tp"),
        P("ep", "tp", None),
        P(None, "tp"),
        P(None, "tp"),
        P("tp", None),
    )
    out_specs = (P("ep", "tp"), P("ep", "tp", None, None), P("ep", None, "tp"))
    return jax.shard_map(
        on_device, mesh=mesh, in_specs=in_specs, out_specs=out_specs, check_vma=False
    )
```

profile of v0, /device:TPU:0, one launch (start us, length us, event | category | flops | bytes accessed | tf_op | source)
XLA Modules:
  0.0 199.6 jit_solution(1012858224445261043)
XLA Ops:
  7.2 0.0 copy-start
  7.2 0.0 copy-start.3
  7.2 0.0 copy-start.4
  7.2 0.0 copy-start.14
  7.2 0.0 copy-start.13
  7.2 0.0 all-reduce.3.cloned.1.call-start
  7.3 1.1 fusion.31
  8.4 0.9 fusion.33
  9.4 0.0 copy-start.8
  9.4 0.0 copy-start.5
  9.4 2.0 fusion.21
  11.4 0.1 reshape.93
  11.5 0.1 convolution_convert_fusion.6
  11.6 0.2 convolution_convert_fusion.5
  11.8 0.0 copy-done.13
  11.8 0.1 subtract_exponential_fusion
  11.9 0.1 copy.59
  12.0 2.0 fusion.22
  14.0 0.0 copy-done.8
  14.1 0.1 reduce_sum.69
  14.1 0.1 copy.58
  14.2 0.1 mul.206
  14.3 30.3 %all-reduce = (bf16[16,512]{1,0:T(8,128)(2,1)S(1)}, bf16[16,512]{1,0:T(8,128)(2,1)S(1)}) all-reduce(bf16[16,512]{1,0:T(8,128)(2,1)S(1)} %convolution_convert_fusion.6, bf16[16,512]{1,0:T(8,128)(2,1)S(1)} %convolution_convert_fusion.5), channel_id=1, replica_groups=mesh['ep'=4,'tp'=8] {'tp'}, use_global_device_ids=true, to_apply=%region_2.0 | all-reduce | flops 16384 | bytes 65536 | tf_op jit(solution)/shard_map/psum | solution.py:80
  44.6 0.1 broadcast_multiply_fusion
  44.7 3.1 %multiply_add_fusion = f32[16,8,64,128]{3,2,1,0:T(8,128)S(1)} fusion(f32[16,8,64,128]{3,2,1,0:T(8,128)} %param.39, f32[16,128]{1,0:T(8,128)S(1)} %get-tuple-element.12, f32[16,8,64]{2,1,0:T(8,128)S(1)} %broadcast_multiply_fusion, f32[16,8]{1,0:T(8,128)S(1)} %copy.58), kind=kLoop, calls=%fused_computation | loop fusion | flops 3145728 | bytes 8430080 | tf_op jit(solution)/shard_map/add | solution.py:102
  47.8 0.0 copy-start.1
  47.8 0.0 copy-start.11
  47.8 9.8 %fusion.68 = f32[16,1,8,64]{3,1,2,0:T(1,128)S(1)} fusion(f32[16,8,64,128]{3,2,1,0:T(8,128)S(1)} %multiply_add_fusion, f32[16,128,1,1]{1,2,3,0:T(1,128)S(1)} %bitcast.72), kind=kOutput, calls=%fused_computation.95 | convolution fusion | flops 12582912 | bytes 4235264 | tf_op jit(solution)/shard_map/shpn,sn->shp/dot_general | solution.py:105
  57.6 0.0 copy-start.2
  57.7 0.0 copy-start.6
  57.7 0.2 multiply_reduce_fusion.1
  57.9 0.1 multiply_convert_fusion
  58.0 0.1 reshape.89
  58.1 2.6 %convolution_convert_fusion.3 = bf16[16,2048]{1,0:T(8,128)(2,1)} fusion(bf16[16,512]{1,0:T(8,128)(2,1)S(1)} %reshape.89, bf16[512,2048]{1,0:T(8,128)(2,1)} %param.42), kind=kOutput, calls=%fused_computation.5 | convolution fusion | flops 33587200 | bytes 2179072 | tf_op jit(solution)/shard_map/dot_general | solution.py:110
  60.7 0.0 all-reduce.3.cloned.1.call-update
  60.7 0.0 reduce-scatter.5.cloned.1.call-start
  60.7 0.1 copy.60
  60.8 0.1 eq.20
  60.9 0.1 fusion.42
  61.0 0.1 reduce_window_sum.11
  61.1 0.2 select_reduce_fusion.1
  61.3 0.1 reduce_sum.73
  61.4 0.1 copy.61
  61.5 0.1 convert_reduce_fusion
  61.5 52.3 %all-reduce.3.cloned.1.call-done = bf16[16,2048]{1,0:T(8,128)(2,1)} async-done(((bf16[16,2048]{1,0:T(8,128)(2,1)}), bf16[16,2048]{1,0:T(8,128)(2,1)}) %all-reduce.3.cloned.1.call-update) | async-done | bytes 65552 | tf_op jit(solution)/shard_map/psum | solution.py:111
  113.9 1.0 fusion.28
  114.9 0.3 convolution_convert_fusion.1
  115.2 10.6 %all_to_all.10 = bf16[4,2,16,2048]{3,2,1,0:T(8,128)(2,1)S(1)} all-to-all(bf16[4,2,16,2048]{3,2,1,0:T(8,128)(2,1)S(1)} %bitcast.69), channel_id=1, replica_groups=mesh['ep'=4,'tp'=8] {'ep'}, dimensions={0} | all-to-all | bytes 1048576 | tf_op jit(solution)/shard_map/all_to_all | solution.py:134
  125.8 2.1 %fusion.7 = f32[4,2,16,256]{3,2,0,1:T(8,128)S(1)} fusion(bf16[2,2048,256]{2,1,0:T(8,128)(2,1)} %param.44, bf16[4,2,16,2048]{3,2,1,0:T(8,128)(2,1)S(1)} %all_to_all.10), kind=kOutput, calls=%fused_computation.12 | convolution fusion | flops 134217728 | bytes 2752512 | tf_op jit(solution)/shard_map/ajcd,jdf->ajcf/dot_general | solution.py:30
  127.8 0.0 copy-done
  127.8 3.3 %fusion = bf16[4,2,16,2048]{3,2,0,1:T(8,128)(2,1)} fusion(bf16[2,256,2048]{2,1,0:T(8,128)(2,1)S(1)} %copy-done, bf16[2,2048,256]{2,1,0:T(8,128)(2,1)} %param.45, bf16[4,2,16,2048]{3,2,1,0:T(8,128)(2,1)S(1)} %all_to_all.10, f32[4,2,16,256]{3,2,0,1:T(8,128)S(1)} %fusion.7), kind=kOutput, calls=%fused_computation.3 | convolution fusion | flops 268894208 | bytes 5373952 | tf_op jit(solution)/shard_map/ajcf,jfd->ajcd/dot_general | solution.py:37
  131.1 0.0 reduce-scatter.5.cloned.1.call-update
  131.1 0.0 reduce-scatter.3.cloned.1.call-start
  131.2 1.5 fusion.65
  132.7 2.9 %fusion.1 = bf16[1,1,16,2048]{3,2,1,0:T(8,128)(2,1)} fusion(bf16[256,2048]{1,0:T(8,128)(2,1)} %param.49, bf16[2048,256]{1,0:T(8,128)(2,1)} %param.48, f32[16,256]{1,0:T(8,128)S(1)} %fusion.65, bf16[16,2048]{1,0:T(8,128)(2,1)S(1)} %get-tuple-element.6, f32[2048]{0:T(1024)S(1)} %copy-done.6, f32[16]{0:T(128)S(1)} %add_rsqrt_fusion.1), kind=kOutput, calls=%fused_computation.6 | convolution fusion | flops 33742848 | bytes 2252864 | tf_op jit(solution)/shard_map/dot_general | solution.py:119
  135.6 0.0 reduce-scatter.3.cloned.1.call-update
  135.7 0.1 select_reduce_fusion
  135.8 25.0 %reduce-scatter.5.cloned.1.call-done = bf16[4,2,16,256]{3,2,0,1:T(8,128)(2,1)} async-done(((bf16[4,2,16,2048]{3,2,0,1:T(8,128)(2,1)}), bf16[4,2,16,256]{3,2,0,1:T(8,128)(2,1)}) %reduce-scatter.5.cloned.1.call-update) | async-done | bytes 65552 | tf_op jit(solution)/shard_map/reduce_scatter | solution.py:140
  160.8 1.5 copy.64
  162.2 3.6 %all-to-all-start.1 = ((bf16[4,2,16,256]{3,2,1,0:T(8,128)(2,1)}), bf16[4,2,16,256]{3,2,1,0:T(8,128)(2,1)S(1)}, u32[]{:S(2)}, u32[]{:S(2)}) async-start(bf16[4,2,16,256]{3,2,1,0:T(8,128)(2,1)} %copy.64), calls=%async_computation.3 | async-start | bytes 131072 | tf_op jit(solution)/shard_map/all_to_all | solution.py:151
  165.9 0.6 fusion.41
  166.5 25.2 %reduce-scatter.3.cloned.1.call-done = bf16[1,1,16,256]{3,2,1,0:T(8,128)(2,1)} async-done(((bf16[1,1,16,2048]{3,2,1,0:T(8,128)(2,1)}), bf16[1,1,16,256]{3,2,1,0:T(8,128)(2,1)}) %reduce-scatter.3.cloned.1.call-update) | async-done | bytes 8208 | tf_op jit(solution)/shard_map/reduce_scatter | solution.py:143
  191.7 0.0 all-to-all-done.1
  191.7 1.4 fusion.24
  (26 shorter events, 0.1 us)
Async XLA Ops:
  7.2 120.7 %copy-start = (bf16[2,256,2048]{2,1,0:T(8,128)(2,1)S(1)}, bf16[2,256,2048]{2,1,0:T(8,128)(2,1)}, u32[]{:S(2)}) copy-start(bf16[2,256,2048]{2,1,0:T(8,128)(2,1)} %param.46) | copy-start | bytes 6291460
  7.2 4.3 %copy-start.3 = (bf16[256,512]{1,0:T(8,128)(2,1)S(1)}, bf16[256,512]{1,0:T(8,128)(2,1)}, u32[]{:S(2)}) copy-start(bf16[256,512]{1,0:T(8,128)(2,1)} %param.32) | copy-start | bytes 786436
  7.2 4.4 %copy-start.4 = (bf16[256,512]{1,0:T(8,128)(2,1)S(1)}, bf16[256,512]{1,0:T(8,128)(2,1)}, u32[]{:S(2)}) copy-start(bf16[256,512]{1,0:T(8,128)(2,1)} %param.33) | copy-start | bytes 786436
  7.2 4.6 %copy-start.14 = (f32[8]{0:T(128)S(1)}, f32[8]{0:T(128)}, u32[]{:S(2)}) copy-start(f32[8]{0:T(128)} %param.35) | copy-start | bytes 100
  7.2 4.6 %copy-start.13 = (f32[16,8]{0,1:T(8,128)S(1)}, f32[16,8]{0,1:T(8,128)}, u32[]{:S(2)}) copy-start(f32[16,8]{0,1:T(8,128)} %param.36) | copy-start | bytes 1540
  7.2 4.6 %copy-start.15 = (f32[8]{0:T(128)S(1)}, f32[8]{0:T(128)}, u32[]{:S(2)}) copy-start(f32[8]{0:T(128)} %param.34) | copy-start | bytes 100
  7.2 4.6 %copy-start.12 = (bf16[2048,8]{0,1:T(8,128)(2,1)S(1)}, bf16[2048,8]{0,1:T(8,128)(2,1)}, u32[]{:S(2)}) copy-start(bf16[2048,8]{0,1:T(8,128)(2,1)} %param.31) | copy-start | bytes 98308
  7.2 106.6 %all-reduce.3.cloned.1.call-start = ((), (), s32[]{:S(2)}) async-start(), calls=%async_computation.4 | async-start | bytes 131072 | tf_op jit(solution)/shard_map/psum | solution.py:111
  9.4 4.6 %copy-start.8 = (bf16[4,512]{1,0:T(4,128)(2,1)S(1)}, bf16[4,512]{1,0:T(4,128)(2,1)}, u32[]{:S(2)}) copy-start(bf16[4,512]{1,0:T(4,128)(2,1)} %param.37) | copy-start | bytes 12292
  9.4 4.7 %copy-start.5 = (bf16[16,3,512]{2,0,1:T(8,128)(2,1)S(1)}, bf16[16,3,512]{2,0,1:T(8,128)(2,1)}, u32[]{:S(2)}) copy-start(bf16[16,3,512]{2,0,1:T(8,128)(2,1)} %param.38) | copy-start | bytes 147460
  11.4 2.8 %copy-start.9 = (f32[512]{0:T(512)S(1)}, f32[512]{0:T(512)}, u32[]{:S(2)}) copy-start(f32[512]{0:T(512)} %param.41) | copy-start | bytes 6148
  47.8 9.8 %copy-start.1 = (f32[16,8,64,128]{3,2,1,0:T(8,128)}, f32[16,8,64,128]{3,2,1,0:T(8,128)S(1)}, u32[]{:S(2)}) copy-start(f32[16,8,64,128]{3,2,1,0:T(8,128)S(1)} %multiply_add_fusion) | copy-start | bytes 12582916
  47.8 9.9 %copy-start.11 = (f32[8]{0:T(128)S(1)}, f32[8]{0:T(128)}, u32[]{:S(2)}) copy-start(f32[8]{0:T(128)} %param.40) | copy-start | bytes 100
  57.6 3.1 %copy-start.7 = (s32[16,4]{0,1:T(4,128)S(1)}, s32[16,4]{0,1:T(4,128)}, u32[]{:S(2)}) copy-start(s32[16,4]{0,1:T(4,128)} %param.26) | copy-start | bytes 772
  57.6 56.2 %copy-start.2 = (bf16[16,2048]{1,0:T(8,128)(2,1)S(1)}, bf16[16,2048]{1,0:T(8,128)(2,1)}, u32[]{:S(2)}) copy-start(bf16[16,2048]{1,0:T(8,128)(2,1)} %param.25) | copy-start | bytes 196612
  57.7 57.2 %copy-start.6 = (f32[2048]{0:T(1024)S(1)}, f32[2048]{0:T(1024)}, u32[]{:S(2)}) copy-start(f32[2048]{0:T(1024)} %param.43) | copy-start | bytes 24580
  60.7 100.1 %reduce-scatter.5.cloned.1.call-start = ((), (), s32[]{:S(2)}) async-start(), calls=%async_computation.6 | async-start | bytes 589824 | tf_op jit(solution)/shard_map/reduce_scatter | solution.py:140
  131.1 4.6 %copy-start.10 = (f32[16,4]{0,1:T(4,128)S(1)}, f32[16,4]{0,1:T(4,128)}, u32[]{:S(2)}) copy-start(f32[16,4]{0,1:T(4,128)} %param.27) | copy-start | bytes 772
  131.1 60.5 %reduce-scatter.3.cloned.1.call-start = ((), (), s32[]{:S(2)}) async-start(), calls=%async_computation.5 | async-start | bytes 73728 | tf_op jit(solution)/shard_map/reduce_scatter | solution.py:143
  162.2 29.4 %all-to-all-start.1 = ((bf16[4,2,16,256]{3,2,1,0:T(8,128)(2,1)}), bf16[4,2,16,256]{3,2,1,0:T(8,128)(2,1)S(1)}, u32[]{:S(2)}, u32[]{:S(2)}) async-start(bf16[4,2,16,256]{3,2,1,0:T(8,128)(2,1)} %copy.64), calls=%async_computation.3 | async-start | bytes 131072 | tf_op jit(solution)/shard_map/all_to_all | solution.py:151
Sparse Core Ops, SparseCore 0:
  60.8 53.0 all-reduce.2
  131.3 29.4 reduce-scatter.4
  163.0 28.6 reduce-scatter.2
where the time goes:
time: 200 us
  waiting for transfers between devices  103 us (52%)
  blocking collectives  40.9 us (20%)
  matrix products  28.4 us (14%)
  between operations  14 us (7%)
  other arithmetic  7.67 us (4%)
  starting transfers between devices  3.77 us (2%)
  local copies, waits for them, and re-layouts  2.39 us (1%)
    psum x1, waiting for transfers between devices, on_device(): mixed = lax.psum(mixer_part.astype(jnp.bfloat16), 'tp')  52.3 us
    psum x1, blocking collectives, on_device(): lax.psum(write_part.astype(jnp.bfloat16), 'tp').astype(jnp.float32)  30.3 us
    reduce_scatter x1, waiting for transfers between devices, on_device(): lax.psum_scatter(shared_part.reshape(1, 1, seq_rows, model_width).astype(...  25.2 us
    reduce_scatter x1, waiting for transfers between devices, on_device(): lax.psum_scatter(terms.astype(jnp.bfloat16), 'tp', scatter_dimension=3, t...  25 us
    all_to_all x1, blocking collectives, on_device(): lax.all_to_all(send_rows, 'ep', split_axis=0, concat_axis=0, tiled=True)  10.6 us
    dot_general x1, matrix products, on_device(): jnp.einsum('shpn,sn->shp', new_state, read_vec, precision=lax.Precision.H...  9.81 us
  transfers between devices with their start and end apart: 4, of which 3 were waited for; matrix products, arithmetic and copies ran while one was open for 4% of the time, Pallas kernels for 0%

commit v1 on v0

v1 whole, which is shorter than its diff:
```python
import functools

import jax
import jax.numpy as jnp
from jax import lax
from jax.experimental import pallas as pl
from jax.experimental.pallas import tpu as pltpu
from jax.sharding import PartitionSpec as P

HEADS = 64
HEAD_DIM = 64
GROUPS = 4
STATE = 128

EPS = 1e-06
F32 = jnp.float32
BF16 = jnp.bfloat16
MESH = pl.DeviceIdType.MESH
VMEM_LIMIT = 56 * 1024 * 1024


def dot(a, b):
    return jnp.dot(a, b, preferred_element_type=F32)


def dot_nt(a, b):
    return lax.dot_general(a, b, (((1,), (1,)), ((), ())), preferred_element_type=F32)


def split(v):
    high = v.astype(BF16)
    return high, (v - high.astype(F32)).astype(BF16)


def softplus(v):
    return jnp.maximum(v, 0.0) + jnp.log1p(jnp.exp(-jnp.abs(v)))


def project_kernel(
    n_tp,
    heads_here,
    tokens_ref,
    gain_ref,
    step_ref,
    gate_hbm,
    input_hbm,
    write_hbm,
    read_hbm,
    vec_ref,
    gate_ref,
    input_ref,
    raw_ref,
    gate_buf,
    input_buf,
    write_buf,
    read_buf,
    normed_buf,
    out_buf,
    in_buf,
    load_sem,
    send_sem,
    recv_sem,
):
    ep = lax.axis_index("ep")
    tp = lax.axis_index("tp")
    loads = [
        pltpu.make_async_copy(src, dst, load_sem.at[i])
        for i, (src, dst) in enumerate(
            (
                (write_hbm, write_buf),
                (read_hbm, read_buf),
                (input_hbm, input_buf),
                (gate_hbm, gate_buf),
            )
        )
    ]
    for load in loads:
        load.start()
    barrier = pltpu.get_barrier_semaphore()

    def greet(k, carry):
        pl.semaphore_signal(
            barrier, inc=1, device_id=(ep, lax.rem(tp + k, n_tp)), device_id_type=MESH
        )
        return carry

    lax.fori_loop(1, n_tp, greet, 0)
    tokens = tokens_ref[...].astype(F32)
    scale = lax.rsqrt(jnp.mean(tokens * tokens, axis=-1, keepdims=True) + EPS)
    normed_buf[...] = (tokens * scale * gain_ref[...]).astype(BF16)
    features = write_buf.shape[0]
    own = normed_buf[:, pl.ds(pl.multiple_of(tp * features, features), features)]
    loads[0].wait()
    loads[1].wait()
    write_part = dot(own, write_buf[...]).astype(BF16)
    read_part = dot(own, read_buf[...]).astype(BF16)
    for g in range(GROUPS):
        out_buf[g, :, :STATE] = write_part[:, g * STATE : (g + 1) * STATE]
        out_buf[g, :, STATE:] = read_part[:, g * STATE : (g + 1) * STATE]
    per_group = HEADS // GROUPS
    pl.semaphore_wait(barrier, n_tp - 1)

    def copy_to(k):
        peer = lax.rem(tp + k, n_tp)
        return pltpu.make_async_remote_copy(
            src_ref=out_buf.at[(peer * heads_here) // per_group],
            dst_ref=in_buf.at[tp],
            send_sem=send_sem.at[peer],
            recv_sem=recv_sem.at[tp],
            device_id=(ep, peer),
            device_id_type=MESH,
        )

    def copy_from(k):
        peer = lax.rem(tp + k, n_tp)
        return pltpu.make_async_remote_copy(
            src_ref=out_buf.at[0],
            dst_ref=in_buf.at[peer],
            send_sem=send_sem.at[peer],
            recv_sem=recv_sem.at[peer],
            device_id=(ep, peer),
            device_id_type=MESH,
        )

    def send(k, carry):
        copy_to(k).start()
        return carry

    lax.fori_loop(1, n_tp, send, 0)
    in_buf[tp] = out_buf[(tp * heads_here) // per_group]
    normed = normed_buf[...]
    raw_ref[...] = dot_nt(step_ref[...], normed)
    loads[2].wait()
    input_ref[...] = dot(normed, input_buf[...]).astype(BF16)
    loads[3].wait()
    gate_ref[...] = dot(normed, gate_buf[...]).astype(BF16)

    def receive(k, carry):
        copy_from(k).wait_recv()
        return carry

    lax.fori_loop(1, n_tp, receive, 0)
    vec_ref[...] = jax.nn.silu(jnp.sum(in_buf[...].astype(F32), axis=0))

    def sent(k, carry):
        copy_to(k).wait_send()
        return carry

    lax.fori_loop(1, n_tp, sent, 0)


def state_kernel(
    bias_ref,
    rate_ref,
    skip_ref,
    vec_ref,
    gate_ref,
    input_ref,
    raw_ref,
    jolt_ref,
    taps_ref,
    filter_ref,
    gain_ref,
    state_hbm,
    weight_hbm,
    part_ref,
    new_hbm,
    new_filter_ref,
    state_buf,
    new_buf,
    weight_buf,
    decay_buf,
    x_buf,
    read_buf,
    load_sem,
    store_sem,
    weight_sem,
):
    rows, width, _ = state_buf.shape
    heads = jolt_ref.shape[0]
    for s in range(rows):
        pltpu.make_async_copy(state_hbm.at[s], state_buf.at[s], load_sem.at[s]).start()
    weight_load = pltpu.make_async_copy(weight_hbm, weight_buf, weight_sem)
    weight_load.start()
    taps = taps_ref[...].astype(F32)
    last = filter_ref.shape[0]
    inputs = input_ref[...]
    total = inputs.astype(F32) * taps[last : last + 1]
    for i in range(last):
        total = total + filter_ref[i].astype(F32) * taps[i : i + 1]
        new_filter_ref[i] = filter_ref[i + 1] if i + 1 < last else inputs
    filtered = jax.nn.silu(total)
    pad = jnp.zeros((128 - rows, width), F32)
    filtered_t = jnp.transpose(jnp.concatenate([filtered, pad], axis=0))[:, :rows]
    head_ids = lax.broadcasted_iota(jnp.int32, (heads, rows), 0)
    bias = jnp.zeros((heads, rows), F32)
    rate = jnp.zeros((heads, rows), F32)
    for h in range(heads):
        bias = jnp.where(head_ids == h, bias_ref[h], bias)
        rate = jnp.where(head_ids == h, rate_ref[h], rate)
    step = softplus(raw_ref[...] + bias)
    decay = jnp.exp(jolt_ref[...] - jnp.exp(rate) * step)

    def expand(v):
        return jnp.concatenate(
            [jnp.broadcast_to(v[h : h + 1], (HEAD_DIM, rows)) for h in range(heads)], axis=0
        )

    decay_buf[...] = expand(decay)
    x_buf[...] = expand(step) * filtered_t
    for s in range(rows):
        pltpu.make_async_copy(state_hbm.at[s], state_buf.at[s], load_sem.at[s]).wait()
        write = vec_ref[s : s + 1, :STATE]
        new = decay_buf[:, s : s + 1] * state_buf[s] + x_buf[:, s : s + 1] * write
        new_buf[s] = new
        pltpu.make_async_copy(new_buf.at[s], new_hbm.at[s], store_sem.at[s]).start()
        read_high, read_low = split(vec_ref[s : s + 1, STATE:])
        high, low = split(new)
        read_buf[s : s + 1, :] = (
            dot_nt(read_high, high) + dot_nt(read_low, high) + dot_nt(read_high, low)
        )
    lane_head = lax.broadcasted_iota(jnp.int32, (1, width), 1) // HEAD_DIM
    skip = jnp.zeros((1, width), F32)
    for h in range(heads):
        skip = jnp.where(lane_head == h, skip_ref[h], skip)
    value = (read_buf[...] + skip * filtered) * jax.nn.silu(gate_ref[...].astype(F32))
    same = (
        lax.broadcasted_iota(jnp.int32, (width, width), 0) // HEAD_DIM
        == lax.broadcasted_iota(jnp.int32, (width, width), 1) // HEAD_DIM
    )
    block = jnp.where(same, 1.0, 0.0).astype(BF16)
    high, low = split(value * value)
    mean_square = (dot(high, block) + dot(low, block)) * (1.0 / HEAD_DIM)
    gated = (value * lax.rsqrt(mean_square + EPS) * gain_ref[...]).astype(BF16)
    weight_load.wait()
    columns = part_ref.shape[2]
    for t in range(part_ref.shape[0]):
        part_ref[t] = dot(gated, weight_buf[:, t * columns : (t + 1) * columns]).astype(BF16)
    for s in range(rows):
        pltpu.make_async_copy(new_buf.at[s], new_hbm.at[s], store_sem.at[s]).wait()


def expert_kernel(
    n_ep,
    n_tp,
    part_ref,
    tokens_ref,
    routes_ref,
    route_weight_ref,
    gain_ref,
    gate_hbm,
    up_hbm,
    down_hbm,
    sgate_hbm,
    sup_hbm,
    sdown_hbm,
    out_ref,
    gate_buf,
    up_buf,
    down_buf,
    sgate_buf,
    sup_buf,
    sdown_buf,
    mix_buf,
    resid_buf,
    share_buf,
    normed_buf,
    total_buf,
    term_buf,
    back_buf,
    load_sem,
    mix_send,
    mix_recv,
    share_send,
    share_recv,
    resid_send,
    resid_recv,
    back_send,
    back_recv,
):
    ep = lax.axis_index("ep")
    tp = lax.axis_index("tp")
    me = ep * n_tp + tp
    n_all = n_ep * n_tp
    rows, columns = out_ref.shape
    loads = [
        pltpu.make_async_copy(src, dst, load_sem.at[i])
        for i, (src, dst) in enumerate(
            (
                (sgate_hbm, sgate_buf),
                (sup_hbm, sup_buf),
                (gate_hbm, gate_buf),
                (up_hbm, up_buf),
                (sdown_hbm, sdown_buf),
                (down_hbm, down_buf),
            )
        )
    ]
    barrier = pltpu.get_barrier_semaphore()

    def place(k):
        other = lax.rem(me + k, n_all)
        return other // n_tp, lax.rem(other, n_tp)

    def loop(low, high, act):
        def body(k, carry):
            act(k)
            return carry

        lax.fori_loop(low, high, body, 0)

    loop(
        1,
        n_all,
        lambda k: pl.semaphore_signal(barrier, inc=1, device_id=place(k), device_id_type=MESH),
    )
    for load in loads:
        load.start()

    lanes = share_buf.shape[2]
    lane_ids = lax.broadcasted_iota(jnp.int32, (rows, lanes), 1)
    share = jnp.zeros((rows, lanes), F32)
    for k in range(routes_ref.shape[1]):
        share = share + jnp.where(
            routes_ref[:, k : k + 1] == lane_ids, route_weight_ref[:, k : k + 1], 0.0
        )
    share_buf[ep] = share

    def mix_copy(k, slot):
        peer = lax.rem(tp + k, n_tp)
        return pltpu.make_async_remote_copy(
            src_ref=part_ref.at[peer],
            dst_ref=mix_buf.at[tp if slot is None else peer],
            send_sem=mix_send.at[peer],
            recv_sem=mix_recv.at[tp if slot is None else peer],
            device_id=(ep, peer),
            device_id_type=MESH,
        )

    def share_copy(k, slot):
        peer = lax.rem(ep + k, n_ep)
        mine = ep if slot is None else peer
        return pltpu.make_async_remote_copy(
            src_ref=share_buf.at[mine],
            dst_ref=share_buf.at[mine],
            send_sem=share_send.at[peer],
            recv_sem=share_recv.at[mine],
            device_id=(peer, tp),
            device_id_type=MESH,
        )

    def resid_copy(k, slot):
        e, t = place(k)
        at_e, at_t = (ep, tp) if slot is None else (e, t)
        return pltpu.make_async_remote_copy(
            src_ref=resid_buf.at[at_e, at_t],
            dst_ref=resid_buf.at[at_e, at_t],
            send_sem=resid_send.at[e * n_tp + t],
            recv_sem=resid_recv.at[at_e * n_tp + at_t],
            device_id=(e, t),
            device_id_type=MESH,
        )

    def back_copy(e, t, slot):
        at_e, at_t = (ep, tp) if slot is None else (e, t)
        return pltpu.make_async_remote_copy(
            src_ref=term_buf.at[t, e],
            dst_ref=back_buf.at[at_e * n_tp + at_t],
            send_sem=back_send.at[e * n_tp + t],
            recv_sem=back_recv.at[at_e * n_tp + at_t],
            device_id=(e, t),
            device_id_type=MESH,
        )

    pl.semaphore_wait(barrier, n_all - 1)
    loop(1, n_tp, lambda k: mix_copy(k, None).start())
    loop(1, n_ep, lambda k: share_copy(k, None).start())
    mix_buf[tp] = part_ref[tp]
    own_tokens = tokens_ref[:, pl.ds(pl.multiple_of(tp * columns, columns), columns)]
    loop(1, n_tp, lambda k: mix_copy(k, 1).wait_recv())
    mixed = jnp.sum(mix_buf[...].astype(F32), axis=0).astype(BF16)
    resid_own = (own_tokens.astype(F32) + mixed.astype(F32)).astype(BF16)
    resid_buf[ep, tp] = resid_own
    loop(1, n_all, lambda k: resid_copy(k, None).start())

    def normalise(e):
        square = jnp.zeros((rows, columns), F32)
        for t in range(n_tp):
            value = resid_buf[e, t].astype(F32)
            square = square + value * value
        mean_square = jnp.sum(square, axis=-1, keepdims=True) * (1.0 / (n_tp * columns))
        scale = lax.rsqrt(mean_square + EPS)
        for t in range(n_tp):
            at = slice(t * columns, (t + 1) * columns)
            value = resid_buf[e, t].astype(F32) * scale * gain_ref[:, at]
            normed_buf[pl.ds(pl.multiple_of(e * rows, rows), rows), at] = value.astype(BF16)

    loop(
        0, n_all - 1, lambda k: resid_copy(k + 1, 1).wait_recv()
    )
    loop(0, n_ep, normalise)
    normed_own = normed_buf[pl.ds(pl.multiple_of(ep * rows, rows), rows), :]
    loads[0].wait()
    loads[1].wait()
    shared_hidden = (
        jax.nn.silu(dot(normed_own, sgate_buf[...])) * dot(normed_own, sup_buf[...])
    ).astype(BF16)
    loads[2].wait()
    loads[3].wait()
    hidden = []
    for j in range(gate_buf.shape[0]):
        normed = normed_buf[...]
        hidden.append(
            (jax.nn.silu(dot(normed, gate_buf[j])) * dot(normed, up_buf[j])).astype(BF16)
        )
    loop(1, n_ep, lambda k: share_copy(k, 1).wait_recv())
    shares = share_buf[...].reshape(n_ep * rows, lanes)
    all_lanes = lax.broadcasted_iota(jnp.int32, shares.shape, 1)
    local = gate_buf.shape[0]
    scales = [
        jnp.sum(jnp.where(all_lanes == ep * local + j, shares, 0.0), axis=1, keepdims=True)
        for j in range(local)
    ]
    loads[4].wait()
    loads[5].wait()
    for t in range(n_tp):
        at = slice(t * columns, (t + 1) * columns)
        term = scales[0] * dot(hidden[0], down_buf[0, :, at])
        for j in range(1, local):
            term = term + scales[j] * dot(hidden[j], down_buf[j, :, at])
        total_buf[t] = term.reshape(n_ep, rows, columns)
        total_buf[t, ep] = total_buf[t, ep] + dot(shared_hidden, sdown_buf[:, at])
        term_buf[t] = total_buf[t].astype(BF16)

        def give(e):
            @pl.when(e * n_tp + t != me)
            def _():
                back_copy(e, t, None).start()

        loop(0, n_ep, give)
    back_buf[me] = term_buf[tp, ep]

    def others(act):
        def body(k):
            e, t = place(k)
            act(e, t)

        loop(1, n_all, body)

    others(lambda e, t: back_copy(e, t, 1).wait_recv())
    out_ref[...] = (
        resid_buf[ep, tp].astype(F32) + jnp.sum(back_buf[...].astype(F32), axis=0)
    ).astype(BF16)
    loop(1, n_tp, lambda k: mix_copy(k, None).wait_send())
    loop(1, n_ep, lambda k: share_copy(k, None).wait_send())
    loop(1, n_all, lambda k: resid_copy(k, None).wait_send())
    others(lambda e, t: back_copy(e, t, None).wait_send())


def on_device(
    tokens,
    routes,
    route_weight,
    mixer_gain,
    gate_weight,
    input_weight,
    step_weight,
    write_weight,
    read_weight,
    step_bias,
    decay_log,
    decay_jolt,
    filter_taps,
    filter_state,
    scan_state,
    skip_gain,
    head_gain,
    output_weight,
    channel_gain,
    expert_gate,
    expert_up,
    expert_down,
    shared_gate,
    shared_up,
    shared_down,
):
    rows, model = tokens.shape
    n_tp = lax.axis_size("tp")
    n_ep = lax.axis_size("ep")
    n_all = n_tp * n_ep
    columns = model // n_tp
    heads_here = step_bias.shape[0]
    width = gate_weight.shape[1]
    vmem = pl.BlockSpec(memory_space=pltpu.VMEM)
    smem = pl.BlockSpec(memory_space=pltpu.SMEM)
    hbm = pl.BlockSpec(memory_space=pl.ANY)
    dma = pltpu.SemaphoreType.DMA
    shape = jax.ShapeDtypeStruct

    vecs, gate_rows, input_rows, step_raw = pl.pallas_call(
        functools.partial(project_kernel, n_tp, heads_here),
        out_shape=(
            shape((rows, 2 * STATE), F32),
            shape((rows, width), BF16),
            shape((rows, width), BF16),
            shape((heads_here, rows), F32),
        ),
        in_specs=[vmem] * 3 + [hbm] * 4,
        out_specs=(vmem,) * 4,
        scratch_shapes=[
            pltpu.VMEM(gate_weight.shape, BF16),
            pltpu.VMEM(input_weight.shape, BF16),
            pltpu.VMEM(write_weight.shape, BF16),
            pltpu.VMEM(read_weight.shape, BF16),
            pltpu.VMEM((rows, model), BF16),
            pltpu.VMEM((GROUPS, rows, 2 * STATE), BF16),
            pltpu.VMEM((n_tp, rows, 2 * STATE), BF16),
            dma((4,)),
            dma((n_tp,)),
            dma((n_tp,)),
        ],
        compiler_params=pltpu.CompilerParams(
            collective_id=0, has_side_effects=True, vmem_limit_bytes=VMEM_LIMIT
        ),
        name="project",
    )(
        tokens,
        mixer_gain.reshape(1, model),
        step_weight.T,
        gate_weight,
        input_weight,
        write_weight,
        read_weight,
    )

    taps = filter_state.shape[1]
    part, new_state, new_filter = pl.pallas_call(
        state_kernel,
        out_shape=(
            shape((n_tp, rows, columns), BF16),
            shape((rows, width, STATE), F32),
            shape((taps, rows, width), BF16),
        ),
        in_specs=[smem] * 3 + [vmem] * 8 + [hbm] * 2,
        out_specs=(vmem, hbm, vmem),
        scratch_shapes=[
            pltpu.VMEM((rows, width, STATE), F32),
            pltpu.VMEM((rows, width, STATE), F32),
            pltpu.VMEM(output_weight.shape, BF16),
            pltpu.VMEM((width, rows), F32),
            pltpu.VMEM((width, rows), F32),
            pltpu.VMEM((rows, width), F32),
            dma((rows,)),
            dma((rows,)),
            dma,
        ],
        compiler_params=pltpu.CompilerParams(vmem_limit_bytes=VMEM_LIMIT),
        name="state",
    )(
        step_bias,
        decay_log,
        skip_gain,
        vecs,
        gate_rows,
        input_rows,
        step_raw,
        decay_jolt.T,
        filter_taps,
        jnp.transpose(filter_state, (1, 0, 2)),
        head_gain.reshape(1, width),
        scan_state.reshape(rows, width, STATE),
        output_weight,
    )

    experts = expert_gate.shape[0] * n_ep
    lanes = -(-experts // 128) * 128
    layer_out = pl.pallas_call(
        functools.partial(expert_kernel, n_ep, n_tp),
        out_shape=shape((rows, columns), BF16),
        in_specs=[vmem] * 5 + [hbm] * 6,
        out_specs=vmem,
        scratch_shapes=[
            pltpu.VMEM(expert_gate.shape, BF16),
            pltpu.VMEM(expert_up.shape, BF16),
            pltpu.VMEM(expert_down.shape, BF16),
            pltpu.VMEM(shared_gate.shape, BF16),
            pltpu.VMEM(shared_up.shape, BF16),
            pltpu.VMEM(shared_down.shape, BF16),
            pltpu.VMEM((n_tp, rows, columns), BF16),
            pltpu.VMEM((n_ep, n_tp, rows, columns), BF16),
            pltpu.VMEM((n_ep, rows, lanes), F32),
            pltpu.VMEM((n_ep * rows, model), BF16),
            pltpu.VMEM((n_tp, n_ep, rows, columns), F32),
            pltpu.VMEM((n_tp, n_ep, rows, columns), BF16),
            pltpu.VMEM((n_all, rows, columns), BF16),
            dma((6,)),
            dma((n_tp,)),
            dma((n_tp,)),
            dma((n_ep,)),
            dma((n_ep,)),
            dma((n_all,)),
            dma((n_all,)),
            dma((n_all,)),
            dma((n_all,)),
        ],
        compiler_params=pltpu.CompilerParams(
            collective_id=1, has_side_effects=True, vmem_limit_bytes=VMEM_LIMIT
        ),
        name="experts",
    )(
        part,
        tokens,
        routes,
        route_weight,
        channel_gain.reshape(1, model),
        expert_gate,
        expert_up,
        expert_down,
        shared_gate,
        shared_up,
        shared_down,
    )
    return (
        layer_out,
        new_state.reshape(scan_state.shape),
        jnp.transpose(new_filter, (1, 0, 2)),
    )


def solution(mesh):
    in_specs = (
        P("ep", None),
        P("ep", None),
        P("ep", None),
        P(),
        P(None, "tp"),
        P(None, "tp"),
        P(None, "tp"),
        P("tp", None),
        P("tp", None),
        P("tp"),
        P("tp"),
        P("ep", "tp"),
        P(None, "tp"),
        P("ep", None, "tp"),
        P("ep", "tp", None, None),
        P("tp"),
        P("tp"),
        P("tp", None),
        P(),
        P("ep", None, "tp"),
        P("ep", None, "tp"),
        P("ep", "tp", None),
        P(None, "tp"),
        P(None, "tp"),
        P("tp", None),
    )
    out_specs = (P("ep", "tp"), P("ep", "tp", None, None), P("ep", None, "tp"))
    return jax.shard_map(
        on_device, mesh=mesh, in_specs=in_specs, out_specs=out_specs, check_vma=False
    )
```

time: 200 us -> 52.1 us (0.26)
  the two profiles are of different devices: /device:TPU:0 before, /device:TPU:25 now
where the time goes in v1:
time: 52.1 us; the launch traced here: 51.8 us
  Pallas kernels  48.5 us (93%)
  local copies, waits for them, and re-layouts  2.67 us (5%)
  between operations  0.68 us (1%)
    pallas_call x1, Pallas kernels, on_device(): pl.pallas_call(functools.partial(expert_kernel, n_ep, n_tp), out_shape=sh...  30.9 us
    pallas_call x1, Pallas kernels, on_device(): pl.pallas_call(state_kernel, out_shape=(shape((n_tp, rows, columns), BF16...  9.74 us
    pallas_call x1, Pallas kernels, on_device(): pl.pallas_call(functools.partial(project_kernel, n_tp, heads_here), out_s...  7.85 us
    unnamed x7, local copies, waits for them, and re-layouts  2.67 us

profile of v1, /device:TPU:25, one launch (start us, length us, event | category | flops | bytes accessed | tf_op | source)
XLA Modules:
  0.0 51.8 jit_solution(15470216394187259210)
XLA Ops:
  0.6 7.8 %project.1 = (f32[16,256]{1,0:T(8,128)}, bf16[16,512]{1,0:T(8,128)(2,1)}, bf16[16,512]{1,0:T(8,128)(2,1)}, f32[8,16]{1,0:T(8,128)}) custom-call(bf16[16,2048]{1,0:T(8,128)(2,1)} %tokens_ref.3, f32[1,2048]{1,0:T(1,128)} %bitcast.12, bf16[8,2048]{1,0:T(8,128)(2,1)} %bitcast.11, bf16[2048,512]{1,0:T(8,128)(2,1)} %gate_hbm.2, bf16[2048,512]{1,0:T(8,128)(2,1)} %input_hbm.1, ...), custom_call_target="tpu_custom_call" | custom-call | tf_op jit(solution)/shard_map/project/pallas_call | solution.py:500
  8.5 0.0 copy-start
  8.5 0.0 copy-start.1
  8.5 9.7 %state.1 = (bf16[8,16,256]{2,1,0:T(8,128)(2,1)}, f32[16,512,128]{2,1,0:T(8,128)}, bf16[3,16,512]{2,1,0:T(8,128)(2,1)}) custom-call(f32[8]{0:T(128)} %bias_ref.1, f32[8]{0:T(128)} %rate_ref.1, f32[8]{0:T(128)} %skip_ref.1, f32[16,256]{1,0:T(8,128)} %get-tuple-element.10.vec_ref, bf16[16,512]{1,0:T(8,128)(2,1)} %get-tuple-element.11.gate_ref, ...), custom_call_target="tpu_custom_call" | custom-call | tf_op jit(solution)/shard_map/state/pallas_call | solution.py:537
  18.3 0.0 copy-done
  18.3 0.7 %copy.28.routes_ref = s32[16,4]{1,0:T(8,128)} copy(s32[16,4]{0,1:T(4,128)S(1)} %copy-done) | data formatting | bytes 512 | tf_op args[1]
  18.9 0.0 copy-done.1
  19.0 0.7 %copy.29.route_weight_ref = f32[16,4]{1,0:T(8,128)} copy(f32[16,4]{0,1:T(4,128)S(1)} %copy-done.1) | data formatting | bytes 512 | tf_op args[2]
  19.6 30.9 %experts.1 = bf16[16,256]{1,0:T(8,128)(2,1)} custom-call(bf16[8,16,256]{2,1,0:T(8,128)(2,1)} %get-tuple-element.14.part_ref, bf16[16,2048]{1,0:T(8,128)(2,1)} %tokens_ref.3, s32[16,4]{1,0:T(8,128)} %copy.28.routes_ref, f32[16,4]{1,0:T(8,128)} %copy.29.route_weight_ref, f32[1,2048]{1,0:T(1,128)} %bitcast.13, bf16[2,2048,256]{2,1,0:T(8,128)(2,1)} %gate_hbm.3, ...), custom_call_target="tpu_custom_call" | custom-call | tf_op jit(solution)/shard_map/experts/pallas_call | solution.py:577
  50.5 1.3 %copy.31 = bf16[16,256]{1,0:T(8,128)(2,1)} copy(bf16[16,256]{1,0:T(8,128)(2,1)} %experts.1) | data formatting | bytes 16384
Async XLA Ops:
  8.5 9.8 %copy-start = (s32[16,4]{0,1:T(4,128)S(1)}, s32[16,4]{0,1:T(4,128)}, u32[]{:S(2)}) copy-start(s32[16,4]{0,1:T(4,128)} %param.26) | copy-start | bytes 772
  8.5 10.5 %copy-start.1 = (f32[16,4]{0,1:T(4,128)S(1)}, f32[16,4]{0,1:T(4,128)}, u32[]{:S(2)}) copy-start(f32[16,4]{0,1:T(4,128)} %param.27) | copy-start | bytes 772

commit v2 on v1

--- a/solution.py
+++ b/solution.py
@@ -266,6 +266,7 @@
     share_buf,
     normed_buf,
     total_buf,
+    shared_buf,
     term_buf,
     back_buf,
     load_sem,
@@ -289,9 +290,9 @@
             (
                 (sgate_hbm, sgate_buf),
                 (sup_hbm, sup_buf),
+                (sdown_hbm, sdown_buf),
                 (gate_hbm, gate_buf),
                 (up_hbm, up_buf),
-                (sdown_hbm, sdown_buf),
                 (down_hbm, down_buf),
             )
         )
@@ -318,13 +319,14 @@
         load.start()
 
     lanes = share_buf.shape[2]
-    lane_ids = lax.broadcasted_iota(jnp.int32, (rows, lanes), 1)
-    share = jnp.zeros((rows, lanes), F32)
-    for k in range(routes_ref.shape[1]):
+    ids = lax.broadcasted_iota(jnp.int32, (lanes, rows), 0)
+    share = jnp.zeros((lanes, rows), F32)
+    for k in range(routes_ref.shape[0]):
         share = share + jnp.where(
-            routes_ref[:, k : k + 1] == lane_ids, route_weight_ref[:, k : k + 1], 0.0
-        )
-    share_buf[ep] = share
+            routes_ref[k : k + 1, :] == ids, route_weight_ref[k : k + 1, :], 0.0
+        )
+    pad = jnp.zeros((lanes, 128 - rows), F32)
+    share_buf[ep] = jnp.transpose(jnp.concatenate([share, pad], axis=1))[:rows]
 
     def mix_copy(k, slot):
         peer = lax.rem(tp + k, n_tp)
@@ -349,8 +351,7 @@
             device_id_type=MESH,
         )
 
-    def resid_copy(k, slot):
-        e, t = place(k)
+    def resid_copy(e, t, slot):
         at_e, at_t = (ep, tp) if slot is None else (e, t)
         return pltpu.make_async_remote_copy(
             src_ref=resid_buf.at[at_e, at_t],
@@ -381,7 +382,17 @@
     mixed = jnp.sum(mix_buf[...].astype(F32), axis=0).astype(BF16)
     resid_own = (own_tokens.astype(F32) + mixed.astype(F32)).astype(BF16)
     resid_buf[ep, tp] = resid_own
-    loop(1, n_all, lambda k: resid_copy(k, None).start())
+    def own_group(act):
+        loop(1, n_tp, lambda k: act(ep, lax.rem(tp + k, n_tp)))
+
+    def other_groups(act):
+        def body(k):
+            act(lax.rem(ep + 1 + k // n_tp, n_ep), lax.rem(tp + lax.rem(k, n_tp), n_tp))
+
+        loop(0, (n_ep - 1) * n_tp, body)
+
+    own_group(lambda e, t: resid_copy(e, t, None).start())
+    other_groups(lambda e, t: resid_copy(e, t, None).start())
 
     def normalise(e):
         square = jnp.zeros((rows, columns), F32)
@@ -395,10 +406,8 @@
             value = resid_buf[e, t].astype(F32) * scale * gain_ref[:, at]
             normed_buf[pl.ds(pl.multiple_of(e * rows, rows), rows), at] = value.astype(BF16)
 
-    loop(
-        0, n_all - 1, lambda k: resid_copy(k + 1, 1).wait_recv()
-    )
-    loop(0, n_ep, normalise)
+    own_group(lambda e, t: resid_copy(e, t, 1).wait_recv())
+    normalise(ep)
     normed_own = normed_buf[pl.ds(pl.multiple_of(ep * rows, rows), rows), :]
     loads[0].wait()
     loads[1].wait()
@@ -406,7 +415,13 @@
         jax.nn.silu(dot(normed_own, sgate_buf[...])) * dot(normed_own, sup_buf[...])
     ).astype(BF16)
     loads[2].wait()
+    for t in range(n_tp):
+        at = slice(t * columns, (t + 1) * columns)
+        shared_buf[t] = dot(shared_hidden, sdown_buf[:, at])
+    other_groups(lambda e, t: resid_copy(e, t, 1).wait_recv())
+    loop(1, n_ep, lambda k: normalise(lax.rem(ep + k, n_ep)))
     loads[3].wait()
+    loads[4].wait()
     hidden = []
     for j in range(gate_buf.shape[0]):
         normed = normed_buf[...]
@@ -421,7 +436,6 @@
         jnp.sum(jnp.where(all_lanes == ep * local + j, shares, 0.0), axis=1, keepdims=True)
         for j in range(local)
     ]
-    loads[4].wait()
     loads[5].wait()
     for t in range(n_tp):
         at = slice(t * columns, (t + 1) * columns)
@@ -429,7 +443,7 @@
         for j in range(1, local):
             term = term + scales[j] * dot(hidden[j], down_buf[j, :, at])
         total_buf[t] = term.reshape(n_ep, rows, columns)
-        total_buf[t, ep] = total_buf[t, ep] + dot(shared_hidden, sdown_buf[:, at])
+        total_buf[t, ep] = total_buf[t, ep] + shared_buf[t]
         term_buf[t] = total_buf[t].astype(BF16)
 
         def give(e):
@@ -453,7 +467,8 @@
     ).astype(BF16)
     loop(1, n_tp, lambda k: mix_copy(k, None).wait_send())
     loop(1, n_ep, lambda k: share_copy(k, None).wait_send())
-    loop(1, n_all, lambda k: resid_copy(k, None).wait_send())
+    own_group(lambda e, t: resid_copy(e, t, None).wait_send())
+    other_groups(lambda e, t: resid_copy(e, t, None).wait_send())
     others(lambda e, t: back_copy(e, t, None).wait_send())
 
 
@@ -591,6 +606,7 @@
             pltpu.VMEM((n_ep, rows, lanes), F32),
             pltpu.VMEM((n_ep * rows, model), BF16),
             pltpu.VMEM((n_tp, n_ep, rows, columns), F32),
+            pltpu.VMEM((n_tp, rows, columns), F32),
             pltpu.VMEM((n_tp, n_ep, rows, columns), BF16),
             pltpu.VMEM((n_all, rows, columns), BF16),
             dma((6,)),
@@ -610,8 +626,8 @@
     )(
         part,
         tokens,
-        routes,
-        route_weight,
+        routes.T,
+        route_weight.T,
         channel_gain.reshape(1, model),
         expert_gate,
         expert_up,

time: 52.1 us -> 50.5 us (0.969)
  local copies, waits for them, and re-layouts: 2.67 us -> 1.3 us
    unnamed x7 -> x1, local copies, waits for them, and re-layouts: 2.67 us -> 1.3 us
where the time goes in v2:
time: 50.5 us; the launch traced here: 50.2 us
  Pallas kernels  48.2 us (95%)
  local copies, waits for them, and re-layouts  1.3 us (3%)
  between operations  0.66 us (1%)
    pallas_call x1, Pallas kernels, on_device(): pl.pallas_call(functools.partial(expert_kernel, n_ep, n_tp), out_shape=sh...  30.6 us
    pallas_call x1, Pallas kernels, on_device(): pl.pallas_call(state_kernel, out_shape=(shape((n_tp, rows, columns), BF16...  9.74 us
    pallas_call x1, Pallas kernels, on_device(): pl.pallas_call(functools.partial(project_kernel, n_tp, heads_here), out_s...  7.85 us
    unnamed x1, local copies, waits for them, and re-layouts  1.3 us

profile of v2, /device:TPU:25, one launch (start us, length us, event | category | flops | bytes accessed | tf_op | source)
XLA Modules:
  0.0 50.2 jit_solution(1757963905947748010)
XLA Ops:
  0.6 7.8 %project.1 = (f32[16,256]{1,0:T(8,128)}, bf16[16,512]{1,0:T(8,128)(2,1)}, bf16[16,512]{1,0:T(8,128)(2,1)}, f32[8,16]{1,0:T(8,128)}) custom-call(bf16[16,2048]{1,0:T(8,128)(2,1)} %tokens_ref.3, f32[1,2048]{1,0:T(1,128)} %bitcast.14, bf16[8,2048]{1,0:T(8,128)(2,1)} %bitcast.13, bf16[2048,512]{1,0:T(8,128)(2,1)} %gate_hbm.2, bf16[2048,512]{1,0:T(8,128)(2,1)} %input_hbm.1, ...), custom_call_target="tpu_custom_call" | custom-call | tf_op jit(solution)/shard_map/project/pallas_call | solution.py:515
  8.5 9.7 %state.1 = (bf16[8,16,256]{2,1,0:T(8,128)(2,1)}, f32[16,512,128]{2,1,0:T(8,128)}, bf16[3,16,512]{2,1,0:T(8,128)(2,1)}) custom-call(f32[8]{0:T(128)} %bias_ref.1, f32[8]{0:T(128)} %rate_ref.1, f32[8]{0:T(128)} %skip_ref.1, f32[16,256]{1,0:T(8,128)} %get-tuple-element.10.vec_ref, bf16[16,512]{1,0:T(8,128)(2,1)} %get-tuple-element.11.gate_ref, ...), custom_call_target="tpu_custom_call" | custom-call | tf_op jit(solution)/shard_map/state/pallas_call | solution.py:552
  18.2 30.6 %experts.1 = bf16[16,256]{1,0:T(8,128)(2,1)} custom-call(bf16[8,16,256]{2,1,0:T(8,128)(2,1)} %get-tuple-element.14.part_ref, bf16[16,2048]{1,0:T(8,128)(2,1)} %tokens_ref.3, s32[4,16]{1,0:T(4,128)} %bitcast.18, f32[4,16]{1,0:T(4,128)} %bitcast.19, f32[1,2048]{1,0:T(1,128)} %bitcast.15, bf16[2,2048,256]{2,1,0:T(8,128)(2,1)} %gate_hbm.3, ...), custom_call_target="tpu_custom_call" | custom-call | tf_op jit(solution)/shard_map/experts/pallas_call | solution.py:592
  48.9 1.3 %copy.29 = bf16[16,256]{1,0:T(8,128)(2,1)} copy(bf16[16,256]{1,0:T(8,128)(2,1)} %experts.1) | data formatting | bytes 16384
